TPU v7x, 32 devices: a whole 2x2x4 slice. The times are simulated.
32 devices in a mesh: sp: 16 (over z, y, x), tp: 2 (over core).
Axes of the slice: x: 2, y: 2, z: 4, core: 2. Of those that a mesh axis runs over, the one named last changes fastest.
Arguments:
- tokens: bfloat16 [4096, 2048], P('sp', 'tp'), may hold values from -6 to 6
- outer_gate: bfloat16 [2048, 1024], P(None, 'tp'), may hold values from -0.125 to 0.125
- inner_gate: bfloat16 [2048, 1024], P(None, 'tp'), may hold values from -0.125 to 0.125
- conv_input: bfloat16 [2048, 1024], P(None, 'tp'), may hold values from -0.125 to 0.125
- conv_taps: bfloat16 [3, 1024], P(None, 'tp'), may hold values from -3.5 to 3.5
- query_down: bfloat16 [2048, 512], P(None, 'tp'), may hold values from -0.125 to 0.125
- latent_down: bfloat16 [2048, 256], P(None, 'tp'), may hold values from -0.125 to 0.125
- rotary_down: bfloat16 [2048, 32], replicated, may hold values from -5.303301 to 5.303301
- query_gain: float32 [512], replicated, may hold values from 0.1 to 1.9
- latent_gain: float32 [256], replicated, may hold values from 0.1 to 1.9
- query_up: bfloat16 [512, 1536], P(None, 'tp'), may hold values from -0.52734375 to 0.52734375
- latent_up: bfloat16 [256, 2048], P(None, 'tp'), may hold values from -0.75 to 0.75
- conv_project: bfloat16 [1024, 2048], P('tp'), may hold values from -0.1875 to 0.1875
- attend_project: bfloat16 [1024, 2048], P('tp'), may hold values from -0.1875 to 0.1875
Outputs:
- mixed: bfloat16 [4096, 2048], P(('sp', 'tp'))
All inputs are finite; a program needn't handle non-finite values.
Results may differ from a plain program's by a relative error of at most 0.035.
Values may be sent and summed in bfloat16 or wider, within the bound.
A program may use at most 128 MiB of HBM per device.

v0:
```python
import math
import jax
import jax.numpy as jnp
from jax import lax
from jax.sharding import PartitionSpec as P

NOPE = 64
ROPE = 32
VDIM = 64
neg_fill = -1e30
rotary_base = 10000.0
norm_epsilon = 1e-06


def shifted(shard, axis, by):
    length = lax.axis_size(axis)
    pairs = [(i, i + by) for i in range(length) if 0 <= i + by < length]
    return lax.ppermute(shard, axis, pairs)


def rotate(values, positions):
    half = values.shape[-1] // 2
    inverse = rotary_base ** (-(jnp.arange(half, dtype=jnp.float32) * 2.0 / (2 * half)))
    angle = positions[:, None] * inverse[None, :]
    if values.ndim == 3:
        angle = angle[:, None, :]
    cosine = jnp.cos(angle)
    sine = jnp.sin(angle)
    first = values[..., :half]
    second = values[..., half:]
    return jnp.concatenate([first * cosine - second * sine, first * sine + second * cosine], -1)


def rms_scale(latent, gain):
    values = latent.astype(jnp.float32)
    factor = lax.rsqrt(jnp.mean(values * values, -1, keepdims=True) + norm_epsilon)
    return (values * factor * gain).astype(jnp.bfloat16)


def local(
    tokens,
    outer_gate,
    inner_gate,
    conv_input,
    conv_taps,
    query_down,
    latent_down,
    rotary_down,
    query_gain,
    latent_gain,
    query_up,
    latent_up,
    conv_project,
    attend_project,
):
    tok_rows = tokens.shape[0]
    local_heads = query_up.shape[1] // (NOPE + ROPE)
    weights = (outer_gate, inner_gate, conv_input, query_down, latent_down, rotary_down)
    piece = lax.all_gather(tokens, "tp", axis=1, tiled=True)
    outer, inner, signal, query_part, latent_part, rotary_raw = tuple(
        (jnp.dot(piece, weight, preferred_element_type=jnp.float32) for weight in weights)
    )
    query_lat, latent_lat = (
        lax.all_gather(query_part.astype(jnp.bfloat16), "tp", axis=1, tiled=True),
        lax.all_gather(latent_part.astype(jnp.bfloat16), "tp", axis=1, tiled=True),
    )
    gated = (inner * signal).astype(jnp.bfloat16)
    reach = conv_taps.shape[0] - 1
    rim = shifted(gated[tok_rows - reach :], "sp", 1)
    padded = jnp.concatenate([rim, gated], 0).astype(jnp.float32)
    taps = conv_taps.astype(jnp.float32)
    filtered = padded[0:tok_rows] * taps[0]
    for index in range(1, reach + 1):
        filtered = filtered + padded[index : index + tok_rows] * taps[index]
    conv_result = (outer * filtered).astype(jnp.bfloat16)
    seq_index = lax.axis_index("sp")
    offset = seq_index * tok_rows
    query_index = offset + jnp.arange(tok_rows, dtype=jnp.int32)
    positions = query_index.astype(jnp.float32)
    query_norm = rms_scale(query_lat, query_gain)
    latent_norm = rms_scale(latent_lat, latent_gain)
    rotary_key = rotate(rotary_raw, positions).astype(jnp.bfloat16)
    query_full = jnp.dot(query_norm, query_up, preferred_element_type=jnp.float32)
    query_full = query_full.reshape(tok_rows, local_heads, NOPE + ROPE)
    query_plain = query_full[..., :NOPE].astype(jnp.bfloat16)
    query_rot = rotate(query_full[..., NOPE:], positions).astype(jnp.bfloat16)
    scale = (NOPE + ROPE) ** (-0.5)
    query_sets = ((query_plain, query_rot, query_index),)
    set_lasts = tuple((jnp.max(members[2]) for members in query_sets))
    overall_last = set_lasts[0]

    def update(current, members, key_plain, values, rot_block, first, block):
        plain, turned, indices = members
        best, total, accum = current
        scores = jnp.einsum("qhd,khd->hqk", plain, key_plain, preferred_element_type=jnp.float32)
        scores = scores + jnp.einsum(
            "qhr,kr->hqk", turned, rot_block, preferred_element_type=jnp.float32
        )
        scores = scores * scale
        key_index = first + jnp.arange(block, dtype=jnp.int32)
        visible = key_index[None, :] <= indices[:, None]
        scores = jnp.where(visible[None], scores, neg_fill)
        new_best = jnp.maximum(best, jnp.max(scores, -1))
        factor = jnp.exp(best - new_best)
        weight = jnp.exp(scores - new_best[..., None])
        total = total * factor + jnp.sum(weight, -1)
        accum = accum * factor[..., None] + jnp.einsum(
            "hqk,khd->hqd", weight.astype(jnp.bfloat16), values, preferred_element_type=jnp.float32
        )
        return (new_best, total, accum)

    initial = tuple(
        (
            (
                jnp.full((local_heads, members[2].shape[0]), neg_fill, jnp.float32),
                jnp.zeros((local_heads, members[2].shape[0]), jnp.float32),
                jnp.zeros((local_heads, members[2].shape[0], VDIM), jnp.float32),
            )
            for members in query_sets
        )
    )
    carry = initial
    keys_latent = lax.all_gather(latent_norm, "sp", axis=0, tiled=True)
    keys_rot = lax.all_gather(rotary_key, "sp", axis=0, tiled=True)
    count = keys_latent.shape[0]
    block = math.gcd(count, 512)
    latent_blocks = keys_latent.reshape(count // block, block, keys_latent.shape[1])
    rot_blocks = keys_rot.reshape(count // block, block, keys_rot.shape[1])

    def advance(states, inputs):
        latent_block, rot_block, number = inputs
        first = number * block

        def compute(current):
            expanded = jnp.dot(latent_block, latent_up, preferred_element_type=jnp.float32)
            expanded = expanded.astype(jnp.bfloat16).reshape(block, local_heads, NOPE + VDIM)
            key_plain = expanded[..., :NOPE]
            values = expanded[..., NOPE:]
            results = []
            for members, last, state in zip(query_sets, set_lasts, current):
                results.append(
                    lax.cond(
                        first > last,
                        lambda kept: kept,
                        lambda kept, members=members: update(
                            kept, members, key_plain, values, rot_block, first, block
                        ),
                        state,
                    )
                )
            return tuple(results)

        return (lax.cond(first > overall_last, lambda current: current, compute, states), None)

    numbers = jnp.arange(count // block, dtype=jnp.int32)
    carry, unused = lax.scan(advance, carry, (latent_blocks, rot_blocks, numbers))
    states = carry
    outputs = []
    for state in states:
        best, total, accum = state
        rows = accum.shape[1]
        outputs.append(
            (accum / total[..., None])
            .transpose(1, 0, 2)
            .reshape(rows, local_heads * VDIM)
            .astype(jnp.bfloat16)
        )
    attended = outputs[0]
    return lax.psum_scatter(
        (
            jnp.dot(conv_result, conv_project, preferred_element_type=jnp.float32)
            + jnp.dot(attended, attend_project, preferred_element_type=jnp.float32)
        ).astype(jnp.bfloat16),
        "tp",
        scatter_dimension=0,
        tiled=True,
    )


def solution(mesh):
    in_specs = (
        P("sp", "tp"),
        P(None, "tp"),
        P(None, "tp"),
        P(None, "tp"),
        P(None, "tp"),
        P(None, "tp"),
        P(None, "tp"),
        P(),
        P(),
        P(),
        P(None, "tp"),
        P(None, "tp"),
        P("tp", None),
        P("tp", None),
    )
    out_specs = P(("sp", "tp"), None)
    return jax.shard_map(local, mesh=mesh, in_specs=in_specs, out_specs=out_specs, check_vma=False)
```

profile of v0, /device:TPU:0, one launch (start us, length us, event | category | flops | bytes accessed | tf_op | source)
XLA Modules:
  0.0 229.9 jit_solution(8106722850243884223)
XLA Ops:
  7.3 13.4 %all-gather.3.cloned.1.call-done = bf16[256,2048]{1,0:T(8,128)(2,1)} async-done(((bf16[256,1024]{1,0:T(8,128)(2,1)}), bf16[256,2048]{1,0:T(8,128)(2,1)}) %all-gather.3.cloned.1.call-update) | async-done | bytes 1048592 | tf_op jit(solution)/shard_map/all_gather | solution.py:59
  20.7 1.9 convolution_convert_fusion.2
  22.5 1.9 all_gather.16
  26.2 2.4 %fusion.46 = f32[256,512]{1,0:T(8,128)S(1)} fusion(bf16[256,2048]{1,0:T(8,128)(2,1)S(1)} %copy-done.2, bf16[2048,512]{1,0:T(8,128)(2,1)} %param.22), kind=kOutput, calls=%fused_computation.75 | convolution fusion | flops 536870912 | bytes 3670016 | tf_op jit(solution)/shard_map/dot_general | solution.py:61
  29.4 3.8 %collective-permute-start = (bf16[2,512]{1,0:T(2,128)(2,1)S(1)}, bf16[2,512]{1,0:T(2,128)(2,1)S(1)}, u32[]{:S(2)}, u32[]{:S(2)}) collective-permute-start(bf16[2,512]{1,0:T(2,128)(2,1)S(1)} %slice.66), channel_id=1, source_target_pairs={{0,2},{2,4},{4,6},{6,8},{8,10},{10,12},{12,14},{14,16},{16,18},{18... | collective-permute-start | bytes 6152 | tf_op jit(solution)/shard_map/ppermute | solution.py:18
  33.6 2.0 all_gather.18
  36.2 40.8 %all_gather.19 = bf16[4096,32]{0,1:T(8,128)(2,1)S(1)} all-gather(bf16[256,32]{0,1:T(8,128)(2,1)S(1)} %pad_maximum_fusion.1), channel_id=1, replica_groups=mesh['sp'=16,'tp'=2] {'sp'}, dimensions={0}, use_global_device_ids=true | all-gather | bytes 278528 | tf_op jit(solution)/shard_map/all_gather | solution.py:124
  78.5 0.9 maximum_convert_fusion
  79.4 4.7 %fusion.24 = f32[256,2048]{1,0:T(8,128)} fusion(bf16[512,2048]{1,0:T(8,128)(2,1)S(1)} %copy-done, bf16[256,2048]{1,0:T(8,128)(2,1)S(1)} %copy-done.2, bf16[2048,512]{1,0:T(8,128)(2,1)} %param.21, f32[258,512]{1,0:T(8,128)} %maximum_convert_fusion, f32[512]{0:T(512)S(1)} %bitcast.60, f32[512]{0:T(512)S(1)} %bitcast.59, f32[512]{0:T(512)S(1)} %bitcast.58), kind=kOutput, calls=%fused_computation.32 | convolution fusion | flops 1074659328 | bytes 8919040 | tf_op jit(solution)/shard_map/dot_general | solution.py:171
  84.1 3.9 %all-gather.5.cloned.1.call-done = bf16[4096,256]{1,0:T(8,128)(2,1)} async-done(((bf16[256,256]{1,0:T(8,128)(2,1)}), bf16[4096,256]{1,0:T(8,128)(2,1)}) %all-gather.5.cloned.1.call-update) | async-done | bytes 2097168 | tf_op jit(solution)/shard_map/all_gather | solution.py:123
  88.6 0.8 broadcast_in_dim.24
  89.5 37.1 %while.15 = (s32[]{:T(128)}, f32[8,256]{1,0:T(8,128)S(1)}, f32[8,256]{1,0:T(8,128)S(1)}, f32[8,256,64]{1,2,0:T(8,128)}, s32[8]{0:T(128)}, /*index=5*/s32[]{:T(12...) while((s32[]{:T(128)}, f32[8,256]{1,0:T(8,128)S(1)}, ...), condition=%wide.region_10.11_spmd.clone, body=%wide.region_3.10_spmd.clone.sunk | while | flops 613290752 | bytes 36222520 | solution.py:156
  89.5 1.3 dynamic_slice.39
  92.5 12.1 %conditional.4 = ((f32[8,256]{1,0:T(8,128)S(1)}, f32[8,256]{1,0:T(8,128)S(1)}, f32[8,256,64]{1,2,0:T(8,128)})) conditional(s32[]{:T(128)} %convert_element_type.122, (s32[]{:T(128)}, s32[]{:T(128)}, bf16[8,512,256]{2,1,0:T(8,128)(2,1)}, s32[]{:T(128)}, bf16[256,1024]{1,0:T(8,128)(2,1)}, /*index=5*/s32[]{:T(128)}, bf16[256,8,64]{0,2,1:T(8,128)(2,1)S(1)}, ...), branch_computations={%region_4.8_spmd, %region_9.9_spmd} | conditional | flops 613290752 | bytes 36204816 | solution.py:153
  92.5 1.6 convolution_convert_fusion
  94.1 1.3 broadcast_add_fusion
  96.0 8.7 %conditional = (f32[8,256]{1,0:T(8,128)S(1)}, f32[8,256]{1,0:T(8,128)S(1)}, f32[8,256,64]{1,2,0:T(8,128)}) conditional(s32[]{:T(128)} %convert_element_type.52, (s32[]{:T(128)}, s32[256]{0:T(256)}, bf16[512,1024]{1,0:T(8,128)(2,1)S(1)}, bf16[256,8,64]{0,2,1:T(8,128)(2,1)S(1)}, bf16[8,512,32]{1,2,0:T(8,128)(2,1)}, /*index=5*/s32[]{:T(128)}, ...), branch_computations={%region_5.6_spmd, %region_8.7_spmd} | conditional | flops 344330752 | bytes 34367116 | solution.py:142
  96.0 1.3 copy.22
  97.3 1.8 fusion.13
  99.3 2.0 fusion.44
  101.3 1.1 fusion.5
  102.7 1.2 fusion.9
  104.6 1.3 dynamic_slice.39
  107.8 1.3 dynamic_slice.39
  110.9 1.3 dynamic_slice.39
  114.0 1.3 dynamic_slice.39
  117.2 1.3 dynamic_slice.39
  120.3 1.3 dynamic_slice.39
  123.4 1.3 dynamic_slice.39
  126.5 1.1 divide_convert_fusion
  127.6 3.9 %fusion.21 = bf16[256,2048]{1,0:T(8,128)(2,1)} fusion(f32[256,2048]{1,0:T(8,128)} %fusion.24, bf16[256,512]{0,1:T(8,128)(2,1)S(1)} %bitcast.55, bf16[512,2048]{1,0:T(8,128)(2,1)} %param.33), kind=kOutput, calls=%fused_computation.26 | convolution fusion | flops 537919488 | bytes 5505024 | tf_op jit(solution)/shard_map/dot_general | solution.py:172
  131.6 91.8 %reduce-scatter.2.cloned.1.call-done = bf16[128,2048]{1,0:T(8,128)(2,1)} async-done(((bf16[256,2048]{1,0:T(8,128)(2,1)}), bf16[128,2048]{1,0:T(8,128)(2,1)}) %reduce-scatter.2.cloned.1.call-update) | async-done | bytes 524304 | tf_op jit(solution)/shard_map/reduce_scatter | solution.py:169
  (90 shorter events, 12.2 us)
Async XLA Ops:
  6.5 72.9 %copy-start = (bf16[512,2048]{1,0:T(8,128)(2,1)S(1)}, bf16[512,2048]{1,0:T(8,128)(2,1)}, u32[]{:S(2)}) copy-start(bf16[512,2048]{1,0:T(8,128)(2,1)} %param.32) | copy-start | bytes 6291460
  6.5 18.1 %copy-start.12 = (f32[256]{0:T(256)S(1)}, f32[256]{0:T(256)}, u32[]{:S(2)}) copy-start(f32[256]{0:T(256)} %param.29) | copy-start | bytes 3076
  6.5 19.6 %copy-start.10 = (bf16[3,512]{1,0:T(4,128)(2,1)S(1)}, bf16[3,512]{1,0:T(4,128)(2,1)}, u32[]{:S(2)}) copy-start(bf16[3,512]{1,0:T(4,128)(2,1)} %param.24) | copy-start | bytes 9220
  6.5 14.1 %all-gather.3.cloned.1.call-start = ((), (), s32[]{:S(2)}) async-start(), calls=%async_computation.1 | async-start | bytes 1572864 | tf_op jit(solution)/shard_map/all_gather | solution.py:59
  7.3 80.8 %all-gather.5.cloned.1.call-start = ((), (), s32[]{:S(2)}) async-start(), calls=%async_computation.2 | async-start | bytes 2228224 | tf_op jit(solution)/shard_map/all_gather | solution.py:123
  20.7 5.5 %copy-start.2 = (bf16[256,2048]{1,0:T(8,128)(2,1)S(1)}, bf16[256,2048]{1,0:T(8,128)(2,1)}, u32[]{:S(2)}) copy-start(bf16[256,2048]{1,0:T(8,128)(2,1)} %all-gather.3.cloned.1.call-done) | copy-start | bytes 3145732
  25.4 198.0 %reduce-scatter.2.cloned.1.call-start = ((), (), s32[]{:S(2)}) async-start(), calls=%async_computation.3 | async-start | bytes 1572864 | tf_op jit(solution)/shard_map/reduce_scatter | solution.py:169
  26.1 2.5 %copy-start.5 = (bf16[2048,512]{1,0:T(8,128)(2,1)S(1)}, bf16[2048,512]{1,0:T(8,128)(2,1)}, u32[]{:S(2)}) copy-start(bf16[2048,512]{1,0:T(8,128)(2,1)} %param.23) | copy-start | bytes 6291460
  28.6 4.6 %copy-start.6 = (bf16[2048,256]{1,0:T(8,128)(2,1)S(1)}, bf16[2048,256]{1,0:T(8,128)(2,1)}, u32[]{:S(2)}) copy-start(bf16[2048,256]{1,0:T(8,128)(2,1)} %param.25) | copy-start | bytes 3145732
  29.3 6.3 %copy-start.8 = (bf16[2048,32]{0,1:T(8,128)(2,1)S(1)}, bf16[2048,32]{0,1:T(8,128)(2,1)}, u32[]{:S(2)}) copy-start(bf16[2048,32]{0,1:T(8,128)(2,1)} %param.27) | copy-start | bytes 393220
  29.4 47.8 %copy-start.7 = (bf16[512,768]{1,0:T(8,128)(2,1)S(1)}, bf16[512,768]{1,0:T(8,128)(2,1)}, u32[]{:S(2)}) copy-start(bf16[512,768]{1,0:T(8,128)(2,1)} %param.30) | copy-start | bytes 2359300
  29.4 47.8 %copy-start.11 = (f32[512]{0:T(512)S(1)}, f32[512]{0:T(512)}, u32[]{:S(2)}) copy-start(f32[512]{0:T(512)} %param.28) | copy-start | bytes 6148
  29.4 49.1 %collective-permute-start = (bf16[2,512]{1,0:T(2,128)(2,1)S(1)}, bf16[2,512]{1,0:T(2,128)(2,1)S(1)}, u32[]{:S(2)}, u32[]{:S(2)}) collective-permute-start(bf16[2,512]{1,0:T(2,128)(2,1)S(1)} %slice.66), channel_id=1, source_target_pairs={{0,2},{2,4},{4,6},{6,8},{8,10},{10,12},{12,14},{14,16},{16,18},{18... | collective-permute-start | bytes 6152 | tf_op jit(solution)/shard_map/ppermute | solution.py:18
  97.3 1.8 copy-start.9
  101.3 1.2 copy-start.1
  101.3 1.3 copy-start.3
  103.8 0.8 copy-start.4
Sparse Core Ops, SparseCore 0:
  8.9 11.7 all-gather.2
  25.5 62.4 all-gather.4
  131.7 91.6 reduce-scatter.1
where the time goes:
time: 232 us; the launch traced here: 230 us
  waiting for transfers between devices  110 us (47%)
  blocking collectives  44.7 us (19%)
  matrix products  21.5 us (9%)
  local copies, waits for them, and re-layouts  19.4 us (8%)
  between operations  13.3 us (6%)
  loops' own time  11 us (5%)
  other arithmetic  6.35 us (3%)
  starting transfers between devices  3.85 us (2%)
    reduce_scatter x1, waiting for transfers between devices, local(): lax.psum_scatter((jnp.dot(conv_result, conv_project, preferred_element_ty...  91.8 us
    all_gather x1, blocking collectives, local(): keys_rot = lax.all_gather(rotary_key, 'sp', axis=0, tiled=True)  40.8 us
    all_gather x1, waiting for transfers between devices, local(): piece = lax.all_gather(tokens, 'tp', axis=1, tiled=True)  13.4 us
    dynamic_slice x8, local copies, waits for them, and re-layouts, local(): lax.scan(advance, carry, (latent_blocks, rot_blocks, numbers))  10.2 us
    another operation x1, loops' own time, local(): lax.scan(advance, carry, (latent_blocks, rot_blocks, numbers))  10 us
    dot_general x5, matrix products, local(): jnp.dot(piece, weight, preferred_element_type=jnp.float32)  5.85 us
    dot_general x1, matrix products, local(): jnp.dot(conv_result, conv_project, preferred_element_type=jnp.float32)  4.74 us
  transfers between devices with their start and end apart: 4, of which 3 were waited for; matrix products, arithmetic and copies ran while one was open for 5% of the time, Pallas kernels for 0%

commit v1 on v0

--- a/solution.py
+++ b/solution.py
@@ -121,7 +121,12 @@
     )
     carry = initial
     keys_latent = lax.all_gather(latent_norm, "sp", axis=0, tiled=True)
-    keys_rot = lax.all_gather(rotary_key, "sp", axis=0, tiled=True)
+    ring = [rotary_key]
+    for hop in range(15):
+        ring.append(lax.ppermute(ring[-1], "sp", [(dev, (dev + 1) % 16) for dev in range(16)]))
+    keys_rot = jnp.roll(
+        jnp.concatenate(ring[::-1], axis=0), (lax.axis_index("sp") + 1) * ring[0].shape[0], axis=0
+    )
     count = keys_latent.shape[0]
     block = math.gcd(count, 512)
     latent_blocks = keys_latent.reshape(count // block, block, keys_latent.shape[1])

time: 232 us -> 320 us (1.38)
  waiting for transfers between devices: 110 us -> 211 us
  blocking collectives: 44.7 us -> 3.9 us
  local copies, waits for them, and re-layouts: 19.4 us -> 44.6 us
    ppermute x0 -> x15, waiting for transfers between devices: none -> 89.5 us  [local(): lax.ppermute(ring[-1], 'sp', [(dev, (dev + 1) % 16) for dev in range(16)])]
    all_gather x1 -> x0, blocking collectives: 40.8 us -> none  [local(): keys_rot = lax.all_gather(rotary_key, 'sp', axis=0, tiled=True)]
    unnamed x18 -> x72, local copies, waits for them, and re-layouts: 0.04 us -> 21.7 us
    all_gather x1, waiting for transfers between devices: 3.88 us -> 17.4 us  [local(): keys_latent = lax.all_gather(latent_norm, 'sp', axis=0, tiled=True)]
  transfers between devices with their start and end apart: 4 -> 19, of which waited for: 3 -> 18; matrix products, arithmetic and copies ran while one was open for 5% -> 12% of each run, Pallas kernels for 0% -> 0%
where the time goes in v1:
time: 320 us; the launch traced here: 316 us
  waiting for transfers between devices  211 us (66%)
  local copies, waits for them, and re-layouts  44.6 us (14%)
  matrix products  21.5 us (7%)
  between operations  13.4 us (4%)
  loops' own time  11.3 us (4%)
  other arithmetic  7.26 us (2%)
  blocking collectives  3.9 us (1%)
  starting transfers between devices  3.81 us (1%)
    reduce_scatter x1, waiting for transfers between devices, local(): lax.psum_scatter((jnp.dot(conv_result, conv_project, preferred_element_ty...  91.6 us
    ppermute x15, waiting for transfers between devices, local(): lax.ppermute(ring[-1], 'sp', [(dev, (dev + 1) % 16) for dev in range(16)])  89.5 us
    unnamed x72, local copies, waits for them, and re-layouts  21.7 us
    all_gather x1, waiting for transfers between devices, local(): keys_latent = lax.all_gather(latent_norm, 'sp', axis=0, tiled=True)  17.4 us
    all_gather x1, waiting for transfers between devices, local(): piece = lax.all_gather(tokens, 'tp', axis=1, tiled=True)  11.3 us
    dynamic_slice x8, local copies, waits for them, and re-layouts, local(): lax.scan(advance, carry, (latent_blocks, rot_blocks, numbers))  10.6 us
    another operation x1, loops' own time, local(): lax.scan(advance, carry, (latent_blocks, rot_blocks, numbers))  10.4 us
  transfers between devices with their start and end apart: 19, of which 18 were waited for; matrix products, arithmetic and copies ran while one was open for 12% of the time, Pallas kernels for 0%

profile of v1, /device:TPU:0, one launch (start us, length us, event | category | flops | bytes accessed | tf_op | source)
XLA Modules:
  0.0 316.4 jit_solution(7201544201417426199)
XLA Ops:
  9.4 11.3 %all-gather.3.cloned.1.call-done = bf16[256,2048]{1,0:T(8,128)(2,1)} async-done(((bf16[256,1024]{1,0:T(8,128)(2,1)}), bf16[256,2048]{1,0:T(8,128)(2,1)}) %all-gather.3.cloned.1.call-update) | async-done | bytes 1048592 | tf_op jit(solution)/shard_map/all_gather | solution.py:59
  20.7 1.6 fusion.47
  22.5 1.8 collective-permute-start.1
  24.3 2.6 fusion.46
  27.7 2.2 collective-permute-done.1
  30.4 6.9 %collective-permute-done.2 = bf16[256,32]{0,1:T(8,128)(2,1)S(1)} collective-permute-done((bf16[256,32]{0,1:T(8,128)(2,1)S(1)}, bf16[256,32]{0,1:T(8,128)(2,1)S(1)}, u32[]{:S(2)}, u32[]{:S(2)}) %collective-permute-start.2) | collective-permute-done | bytes 16416 | tf_op jit(solution)/shard_map/ppermute | solution.py:126
  37.7 6.9 %collective-permute-done.3 = bf16[256,32]{0,1:T(8,128)(2,1)S(1)} collective-permute-done((bf16[256,32]{0,1:T(8,128)(2,1)S(1)}, bf16[256,32]{0,1:T(8,128)(2,1)S(1)}, u32[]{:S(2)}, u32[]{:S(2)}) %collective-permute-start.3) | collective-permute-done | bytes 16416 | tf_op jit(solution)/shard_map/ppermute | solution.py:126
  44.6 2.0 all_gather.15
  46.6 5.3 %collective-permute-done.4 = bf16[256,32]{0,1:T(8,128)(2,1)S(1)} collective-permute-done((bf16[256,32]{0,1:T(8,128)(2,1)S(1)}, bf16[256,32]{0,1:T(8,128)(2,1)S(1)}, u32[]{:S(2)}, u32[]{:S(2)}) %collective-permute-start.4) | collective-permute-done | bytes 16416 | tf_op jit(solution)/shard_map/ppermute | solution.py:126
  52.0 7.2 %collective-permute-done.5 = bf16[256,32]{0,1:T(8,128)(2,1)S(1)} collective-permute-done((bf16[256,32]{0,1:T(8,128)(2,1)S(1)}, bf16[256,32]{0,1:T(8,128)(2,1)S(1)}, u32[]{:S(2)}, u32[]{:S(2)}) %collective-permute-start.5) | collective-permute-done | bytes 16416 | tf_op jit(solution)/shard_map/ppermute | solution.py:126
  59.2 7.3 %collective-permute-done.6 = bf16[256,32]{0,1:T(8,128)(2,1)S(1)} collective-permute-done((bf16[256,32]{0,1:T(8,128)(2,1)S(1)}, bf16[256,32]{0,1:T(8,128)(2,1)S(1)}, u32[]{:S(2)}, u32[]{:S(2)}) %collective-permute-start.6) | collective-permute-done | bytes 16416 | tf_op jit(solution)/shard_map/ppermute | solution.py:126
  66.6 1.9 all_gather.13
  68.5 5.4 %collective-permute-done.7 = bf16[256,32]{0,1:T(8,128)(2,1)S(1)} collective-permute-done((bf16[256,32]{0,1:T(8,128)(2,1)S(1)}, bf16[256,32]{0,1:T(8,128)(2,1)S(1)}, u32[]{:S(2)}, u32[]{:S(2)}) %collective-permute-start.7) | collective-permute-done | bytes 16416 | tf_op jit(solution)/shard_map/ppermute | solution.py:126
  74.0 7.2 %collective-permute-done.8 = bf16[256,32]{0,1:T(8,128)(2,1)S(1)} collective-permute-done((bf16[256,32]{0,1:T(8,128)(2,1)S(1)}, bf16[256,32]{0,1:T(8,128)(2,1)S(1)}, u32[]{:S(2)}, u32[]{:S(2)}) %collective-permute-start.8) | collective-permute-done | bytes 16416 | tf_op jit(solution)/shard_map/ppermute | solution.py:126
  81.9 1.9 collective-permute-start
  83.7 4.9 %collective-permute-done.9 = bf16[256,32]{0,1:T(8,128)(2,1)S(1)} collective-permute-done((bf16[256,32]{0,1:T(8,128)(2,1)S(1)}, bf16[256,32]{0,1:T(8,128)(2,1)S(1)}, u32[]{:S(2)}, u32[]{:S(2)}) %collective-permute-start.9) | collective-permute-done | bytes 16416 | tf_op jit(solution)/shard_map/ppermute | solution.py:126
  89.2 6.8 %collective-permute-done.10 = bf16[256,32]{0,1:T(8,128)(2,1)S(1)} collective-permute-done((bf16[256,32]{0,1:T(8,128)(2,1)S(1)}, bf16[256,32]{0,1:T(8,128)(2,1)S(1)}, u32[]{:S(2)}, u32[]{:S(2)}) %collective-permute-start.10) | collective-permute-done | bytes 16416 | tf_op jit(solution)/shard_map/ppermute | solution.py:126
  96.1 7.2 %collective-permute-done.11 = bf16[256,32]{0,1:T(8,128)(2,1)S(1)} collective-permute-done((bf16[256,32]{0,1:T(8,128)(2,1)S(1)}, bf16[256,32]{0,1:T(8,128)(2,1)S(1)}, u32[]{:S(2)}, u32[]{:S(2)}) %collective-permute-start.11) | collective-permute-done | bytes 16416 | tf_op jit(solution)/shard_map/ppermute | solution.py:126
  104.1 6.7 %collective-permute-done.12 = bf16[256,32]{0,1:T(8,128)(2,1)} collective-permute-done((bf16[256,32]{0,1:T(8,128)(2,1)S(1)}, bf16[256,32]{0,1:T(8,128)(2,1)}, u32[]{:S(2)}, u32[]{:S(2)}) %collective-permute-start.12) | collective-permute-done | bytes 16416 | tf_op jit(solution)/shard_map/ppermute | solution.py:126
  112.0 6.5 %collective-permute-done.13 = bf16[256,32]{0,1:T(8,128)(2,1)} collective-permute-done((bf16[256,32]{0,1:T(8,128)(2,1)}, bf16[256,32]{0,1:T(8,128)(2,1)}, u32[]{:S(2)}, u32[]{:S(2)}) %collective-permute-start.13) | collective-permute-done | bytes 16416 | tf_op jit(solution)/shard_map/ppermute | solution.py:126
  118.4 1.8 maximum_convert_fusion
  120.3 5.9 %collective-permute-done.14 = bf16[256,32]{0,1:T(8,128)(2,1)} collective-permute-done((bf16[256,32]{0,1:T(8,128)(2,1)}, bf16[256,32]{0,1:T(8,128)(2,1)}, u32[]{:S(2)}, u32[]{:S(2)}) %collective-permute-start.14) | collective-permute-done | bytes 16416 | tf_op jit(solution)/shard_map/ppermute | solution.py:126
  126.2 4.7 %fusion.24 = f32[256,2048]{1,0:T(8,128)} fusion(bf16[512,2048]{1,0:T(8,128)(2,1)S(1)} %copy-done, bf16[256,2048]{1,0:T(8,128)(2,1)S(1)} %copy-done.2, bf16[2048,512]{1,0:T(8,128)(2,1)} %param.21, f32[258,512]{1,0:T(8,128)} %maximum_convert_fusion, f32[512]{0:T(512)} %bitcast.60, f32[512]{0:T(512)} %bitcast.59, f32[512]{0:T(512)} %bitcast.58), kind=kOutput, calls=%fused_computation.32 | convolution fusion | flops 1074659328 | bytes 8919040 | tf_op jit(solution)/shard_map/dot_general | solution.py:176
  130.9 3.1 collective-permute-done.15
  156.4 17.4 %all-gather.5.cloned.1.call-done = bf16[4096,256]{1,0:T(8,128)(2,1)} async-done(((bf16[256,256]{1,0:T(8,128)(2,1)}), bf16[4096,256]{1,0:T(8,128)(2,1)}) %all-gather.5.cloned.1.call-update) | async-done | bytes 2097168 | tf_op jit(solution)/shard_map/all_gather | solution.py:123
  175.2 38.0 %while.15 = (s32[]{:T(128)}, f32[8,256]{1,0:T(8,128)S(1)}, f32[8,256]{1,0:T(8,128)S(1)}, f32[8,256,64]{1,2,0:T(8,128)}, s32[8]{0:T(128)}, /*index=5*/s32[]{:T(12...) while((s32[]{:T(128)}, f32[8,256]{1,0:T(8,128)S(1)}, ...), condition=%wide.region_10.11_spmd.clone, body=%wide.region_3.10_spmd.clone.sunk | while | flops 613290752 | bytes 36222520 | solution.py:161
  178.4 12.1 %conditional.4 = ((f32[8,256]{1,0:T(8,128)S(1)}, f32[8,256]{1,0:T(8,128)S(1)}, f32[8,256,64]{1,2,0:T(8,128)})) conditional(s32[]{:T(128)} %convert_element_type.122, (s32[]{:T(128)}, s32[]{:T(128)}, bf16[8,512,256]{2,1,0:T(8,128)(2,1)}, s32[]{:T(128)}, bf16[256,1024]{1,0:T(8,128)(2,1)}, /*index=5*/s32[]{:T(128)}, bf16[256,8,64]{0,2,1:T(8,128)(2,1)S(1)}, ...), branch_computations={%region_4.8_spmd, %region_9.9_spmd} | conditional | flops 613290752 | bytes 36204816 | solution.py:158
  181.8 8.7 %conditional = (f32[8,256]{1,0:T(8,128)S(1)}, f32[8,256]{1,0:T(8,128)S(1)}, f32[8,256,64]{1,2,0:T(8,128)}) conditional(s32[]{:T(128)} %convert_element_type.52, (s32[]{:T(128)}, s32[256]{0:T(256)}, bf16[512,1024]{1,0:T(8,128)(2,1)S(1)}, bf16[256,8,64]{0,2,1:T(8,128)(2,1)S(1)}, bf16[8,512,32]{1,2,0:T(8,128)(2,1)}, /*index=5*/s32[]{:T(128)}, ...), branch_computations={%region_5.6_spmd, %region_8.7_spmd} | conditional | flops 344330752 | bytes 34367116 | solution.py:147
  183.2 1.8 fusion.13
  185.2 2.0 fusion.44
  214.4 3.9 %fusion.21 = bf16[256,2048]{1,0:T(8,128)(2,1)} fusion(f32[256,2048]{1,0:T(8,128)} %fusion.24, bf16[256,512]{0,1:T(8,128)(2,1)S(1)} %bitcast.55, bf16[512,2048]{1,0:T(8,128)(2,1)} %param.33), kind=kOutput, calls=%fused_computation.26 | convolution fusion | flops 537919488 | bytes 5505024 | tf_op jit(solution)/shard_map/dot_general | solution.py:177
  218.3 91.6 %reduce-scatter.2.cloned.1.call-done = bf16[128,2048]{1,0:T(8,128)(2,1)} async-done(((bf16[256,2048]{1,0:T(8,128)(2,1)}), bf16[128,2048]{1,0:T(8,128)(2,1)}) %reduce-scatter.2.cloned.1.call-update) | async-done | bytes 524304 | tf_op jit(solution)/shard_map/reduce_scatter | solution.py:174
  (176 shorter events, 56.0 us)
Async XLA Ops:
  6.5 119.6 %copy-start = (bf16[512,2048]{1,0:T(8,128)(2,1)S(1)}, bf16[512,2048]{1,0:T(8,128)(2,1)}, u32[]{:S(2)}) copy-start(bf16[512,2048]{1,0:T(8,128)(2,1)} %param.32) | copy-start | bytes 6291460
  6.5 14.1 %all-gather.3.cloned.1.call-start = ((), (), s32[]{:S(2)}) async-start(), calls=%async_computation.1 | async-start | bytes 1572864 | tf_op jit(solution)/shard_map/all_gather | solution.py:59
  7.3 166.5 %all-gather.5.cloned.1.call-start = ((), (), s32[]{:S(2)}) async-start(), calls=%async_computation.2 | async-start | bytes 2228224 | tf_op jit(solution)/shard_map/all_gather | solution.py:123
  22.5 7.4 %collective-permute-start.1 = (bf16[256,32]{0,1:T(8,128)(2,1)S(1)}, bf16[256,32]{0,1:T(8,128)(2,1)S(1)}, u32[]{:S(2)}, u32[]{:S(2)}) collective-permute-start(bf16[256,32]{0,1:T(8,128)(2,1)S(1)} %pad_maximum_fusion.1), channel_id=1, source_target_pairs={{0,2},{2,4},{4,6},{6,8},{8,10},{10,12},{12,14},{14,16},{16,18},{18... | collective-permute-start | bytes 49160 | tf_op jit(solution)/shard_map/ppermute | solution.py:126
  27.7 53.6 %copy-start.7 = (bf16[256,512]{1,0:T(8,128)(2,1)}, bf16[256,512]{1,0:T(8,128)(2,1)S(1)}, u32[]{:S(2)}) copy-start(bf16[256,512]{1,0:T(8,128)(2,1)S(1)} %fusion.23) | copy-start | bytes 786436
  27.7 61.0 %copy-start.9 = (bf16[512,768]{1,0:T(8,128)(2,1)S(1)}, bf16[512,768]{1,0:T(8,128)(2,1)}, u32[]{:S(2)}) copy-start(bf16[512,768]{1,0:T(8,128)(2,1)} %param.30) | copy-start | bytes 2359300
  27.7 61.0 %copy-start.23 = (f32[512]{0:T(512)S(1)}, f32[512]{0:T(512)}, u32[]{:S(2)}) copy-start(f32[512]{0:T(512)} %param.28) | copy-start | bytes 6148
  29.9 16.7 %copy-start.12 = (bf16[256,32]{0,1:T(8,128)(2,1)}, bf16[256,32]{0,1:T(8,128)(2,1)S(1)}, u32[]{:S(2)}) copy-start(bf16[256,32]{0,1:T(8,128)(2,1)S(1)} %collective-permute-done.1) | copy-start | bytes 49156
  29.9 7.3 %collective-permute-start.2 = (bf16[256,32]{0,1:T(8,128)(2,1)S(1)}, bf16[256,32]{0,1:T(8,128)(2,1)S(1)}, u32[]{:S(2)}, u32[]{:S(2)}) collective-permute-start(bf16[256,32]{0,1:T(8,128)(2,1)S(1)} %collective-permute-done.1), channel_id=1, source_target_pairs={{0,2},{2,4},{4,6},{6,8},{8,10},{10,12},{12,14},{14,16},{16,18},{18... | collective-permute-start | bytes 49160 | tf_op jit(solution)/shard_map/ppermute | solution.py:126
  30.3 73.0 %copy-start.24 = (f32[256]{0:T(256)S(1)}, f32[256]{0:T(256)}, u32[]{:S(2)}) copy-start(f32[256]{0:T(256)} %param.29) | copy-start | bytes 3076
  37.2 52.0 %copy-start.13 = (bf16[256,32]{0,1:T(8,128)(2,1)}, bf16[256,32]{0,1:T(8,128)(2,1)S(1)}, u32[]{:S(2)}) copy-start(bf16[256,32]{0,1:T(8,128)(2,1)S(1)} %collective-permute-done.2) | copy-start | bytes 49156
  37.2 7.3 %collective-permute-start.3 = (bf16[256,32]{0,1:T(8,128)(2,1)S(1)}, bf16[256,32]{0,1:T(8,128)(2,1)S(1)}, u32[]{:S(2)}, u32[]{:S(2)}) collective-permute-start(bf16[256,32]{0,1:T(8,128)(2,1)S(1)} %collective-permute-done.2), channel_id=1, source_target_pairs={{0,2},{2,4},{4,6},{6,8},{8,10},{10,12},{12,14},{14,16},{16,18},{18... | collective-permute-start | bytes 49160 | tf_op jit(solution)/shard_map/ppermute | solution.py:126
  44.6 51.4 %copy-start.14 = (bf16[256,32]{0,1:T(8,128)(2,1)}, bf16[256,32]{0,1:T(8,128)(2,1)S(1)}, u32[]{:S(2)}) copy-start(bf16[256,32]{0,1:T(8,128)(2,1)S(1)} %collective-permute-done.3) | copy-start | bytes 49156
  44.6 7.3 %collective-permute-start.4 = (bf16[256,32]{0,1:T(8,128)(2,1)S(1)}, bf16[256,32]{0,1:T(8,128)(2,1)S(1)}, u32[]{:S(2)}, u32[]{:S(2)}) collective-permute-start(bf16[256,32]{0,1:T(8,128)(2,1)S(1)} %collective-permute-done.3), channel_id=1, source_target_pairs={{0,2},{2,4},{4,6},{6,8},{8,10},{10,12},{12,14},{14,16},{16,18},{18... | collective-permute-start | bytes 49160 | tf_op jit(solution)/shard_map/ppermute | solution.py:126
  51.9 44.1 %copy-start.15 = (bf16[256,32]{0,1:T(8,128)(2,1)}, bf16[256,32]{0,1:T(8,128)(2,1)S(1)}, u32[]{:S(2)}) copy-start(bf16[256,32]{0,1:T(8,128)(2,1)S(1)} %collective-permute-done.4) | copy-start | bytes 49156
  51.9 7.3 %collective-permute-start.5 = (bf16[256,32]{0,1:T(8,128)(2,1)S(1)}, bf16[256,32]{0,1:T(8,128)(2,1)S(1)}, u32[]{:S(2)}, u32[]{:S(2)}) collective-permute-start(bf16[256,32]{0,1:T(8,128)(2,1)S(1)} %collective-permute-done.4), channel_id=1, source_target_pairs={{0,2},{2,4},{4,6},{6,8},{8,10},{10,12},{12,14},{14,16},{16,18},{18... | collective-permute-start | bytes 49160 | tf_op jit(solution)/shard_map/ppermute | solution.py:126
  59.2 36.8 %copy-start.16 = (bf16[256,32]{0,1:T(8,128)(2,1)}, bf16[256,32]{0,1:T(8,128)(2,1)S(1)}, u32[]{:S(2)}) copy-start(bf16[256,32]{0,1:T(8,128)(2,1)S(1)} %collective-permute-done.5) | copy-start | bytes 49156
  59.2 7.3 %collective-permute-start.6 = (bf16[256,32]{0,1:T(8,128)(2,1)S(1)}, bf16[256,32]{0,1:T(8,128)(2,1)S(1)}, u32[]{:S(2)}, u32[]{:S(2)}) collective-permute-start(bf16[256,32]{0,1:T(8,128)(2,1)S(1)} %collective-permute-done.5), channel_id=1, source_target_pairs={{0,2},{2,4},{4,6},{6,8},{8,10},{10,12},{12,14},{14,16},{16,18},{18... | collective-permute-start | bytes 49160 | tf_op jit(solution)/shard_map/ppermute | solution.py:126
  66.6 22.0 %copy-start.17 = (bf16[256,32]{0,1:T(8,128)(2,1)}, bf16[256,32]{0,1:T(8,128)(2,1)S(1)}, u32[]{:S(2)}) copy-start(bf16[256,32]{0,1:T(8,128)(2,1)S(1)} %collective-permute-done.6) | copy-start | bytes 49156
  66.6 7.3 %collective-permute-start.7 = (bf16[256,32]{0,1:T(8,128)(2,1)S(1)}, bf16[256,32]{0,1:T(8,128)(2,1)S(1)}, u32[]{:S(2)}, u32[]{:S(2)}) collective-permute-start(bf16[256,32]{0,1:T(8,128)(2,1)S(1)} %collective-permute-done.6), channel_id=1, source_target_pairs={{0,2},{2,4},{4,6},{6,8},{8,10},{10,12},{12,14},{14,16},{16,18},{18... | collective-permute-start | bytes 49160 | tf_op jit(solution)/shard_map/ppermute | solution.py:126
  73.9 7.3 %collective-permute-start.8 = (bf16[256,32]{0,1:T(8,128)(2,1)S(1)}, bf16[256,32]{0,1:T(8,128)(2,1)S(1)}, u32[]{:S(2)}, u32[]{:S(2)}) collective-permute-start(bf16[256,32]{0,1:T(8,128)(2,1)S(1)} %collective-permute-done.7), channel_id=1, source_target_pairs={{0,2},{2,4},{4,6},{6,8},{8,10},{10,12},{12,14},{14,16},{16,18},{18... | collective-permute-start | bytes 49160 | tf_op jit(solution)/shard_map/ppermute | solution.py:126
  81.3 14.8 %copy-start.19 = (bf16[256,32]{0,1:T(8,128)(2,1)}, bf16[256,32]{0,1:T(8,128)(2,1)S(1)}, u32[]{:S(2)}) copy-start(bf16[256,32]{0,1:T(8,128)(2,1)S(1)} %collective-permute-done.8) | copy-start | bytes 49156
  81.3 7.3 %collective-permute-start.9 = (bf16[256,32]{0,1:T(8,128)(2,1)S(1)}, bf16[256,32]{0,1:T(8,128)(2,1)S(1)}, u32[]{:S(2)}, u32[]{:S(2)}) collective-permute-start(bf16[256,32]{0,1:T(8,128)(2,1)S(1)} %collective-permute-done.8), channel_id=1, source_target_pairs={{0,2},{2,4},{4,6},{6,8},{8,10},{10,12},{12,14},{14,16},{16,18},{18... | collective-permute-start | bytes 49160 | tf_op jit(solution)/shard_map/ppermute | solution.py:126
  81.9 36.6 %collective-permute-start = (bf16[2,512]{1,0:T(2,128)(2,1)}, bf16[2,512]{1,0:T(2,128)(2,1)}, u32[]{:S(2)}, u32[]{:S(2)}) collective-permute-start(bf16[2,512]{1,0:T(2,128)(2,1)} %slice.66), channel_id=1, source_target_pairs={{0,2},{2,4},{4,6},{6,8},{8,10},{10,12},{12,14},{14,16},{16,18},{18... | collective-permute-start | bytes 6152 | tf_op jit(solution)/shard_map/ppermute | solution.py:18
  88.6 7.4 %collective-permute-start.10 = (bf16[256,32]{0,1:T(8,128)(2,1)S(1)}, bf16[256,32]{0,1:T(8,128)(2,1)S(1)}, u32[]{:S(2)}, u32[]{:S(2)}) collective-permute-start(bf16[256,32]{0,1:T(8,128)(2,1)S(1)} %collective-permute-done.9), channel_id=1, source_target_pairs={{0,2},{2,4},{4,6},{6,8},{8,10},{10,12},{12,14},{14,16},{16,18},{18... | collective-permute-start | bytes 49160 | tf_op jit(solution)/shard_map/ppermute | solution.py:126
  96.0 14.8 %copy-start.21 = (bf16[256,32]{0,1:T(8,128)(2,1)}, bf16[256,32]{0,1:T(8,128)(2,1)S(1)}, u32[]{:S(2)}) copy-start(bf16[256,32]{0,1:T(8,128)(2,1)S(1)} %collective-permute-done.10) | copy-start | bytes 49156
  96.0 7.3 %collective-permute-start.11 = (bf16[256,32]{0,1:T(8,128)(2,1)S(1)}, bf16[256,32]{0,1:T(8,128)(2,1)S(1)}, u32[]{:S(2)}, u32[]{:S(2)}) collective-permute-start(bf16[256,32]{0,1:T(8,128)(2,1)S(1)} %collective-permute-done.10), channel_id=1, source_target_pairs={{0,2},{2,4},{4,6},{6,8},{8,10},{10,12},{12,14},{14,16},{16,18},{18... | collective-permute-start | bytes 49160 | tf_op jit(solution)/shard_map/ppermute | solution.py:126
  103.3 7.4 %collective-permute-start.12 = (bf16[256,32]{0,1:T(8,128)(2,1)S(1)}, bf16[256,32]{0,1:T(8,128)(2,1)}, u32[]{:S(2)}, u32[]{:S(2)}) collective-permute-start(bf16[256,32]{0,1:T(8,128)(2,1)S(1)} %collective-permute-done.11), channel_id=1, source_target_pairs={{0,2},{2,4},{4,6},{6,8},{8,10},{10,12},{12,14},{14,16},{16,18},{18... | collective-permute-start | bytes 49160 | tf_op jit(solution)/shard_map/ppermute | solution.py:126
  110.8 7.7 %collective-permute-start.13 = (bf16[256,32]{0,1:T(8,128)(2,1)}, bf16[256,32]{0,1:T(8,128)(2,1)}, u32[]{:S(2)}, u32[]{:S(2)}) collective-permute-start(bf16[256,32]{0,1:T(8,128)(2,1)} %collective-permute-done.12), channel_id=1, source_target_pairs={{0,2},{2,4},{4,6},{6,8},{8,10},{10,12},{12,14},{14,16},{16,18},{18... | collective-permute-start | bytes 49160 | tf_op jit(solution)/shard_map/ppermute | solution.py:126
  111.9 198.0 %reduce-scatter.2.cloned.1.call-start = ((), (), s32[]{:S(2)}) async-start(), calls=%async_computation.3 | async-start | bytes 1572864 | tf_op jit(solution)/shard_map/reduce_scatter | solution.py:174
  118.4 7.8 %collective-permute-start.14 = (bf16[256,32]{0,1:T(8,128)(2,1)}, bf16[256,32]{0,1:T(8,128)(2,1)}, u32[]{:S(2)}, u32[]{:S(2)}) collective-permute-start(bf16[256,32]{0,1:T(8,128)(2,1)} %collective-permute-done.13), channel_id=1, source_target_pairs={{0,2},{2,4},{4,6},{6,8},{8,10},{10,12},{12,14},{14,16},{16,18},{18... | collective-permute-start | bytes 49160 | tf_op jit(solution)/shard_map/ppermute | solution.py:126
  126.2 7.9 %collective-permute-start.15 = (bf16[256,32]{0,1:T(8,128)(2,1)}, bf16[256,32]{0,1:T(8,128)(2,1)}, u32[]{:S(2)}, u32[]{:S(2)}) collective-permute-start(bf16[256,32]{0,1:T(8,128)(2,1)} %collective-permute-done.14), channel_id=1, source_target_pairs={{0,2},{2,4},{4,6},{6,8},{8,10},{10,12},{12,14},{14,16},{16,18},{18... | collective-permute-start | bytes 49160 | tf_op jit(solution)/shard_map/ppermute | solution.py:126
  (12 other events, 64.0 us)
Sparse Core Ops, SparseCore 0:
  8.9 11.7 all-gather.2
  112.0 61.7 all-gather.4
  218.4 91.4 reduce-scatter.1
